TPU v7x, 32 devices: a whole 2x2x4 slice. The times are simulated.
32 devices in a mesh: sp: 16 (over z, y, x), tp: 2 (over core).
Axes of the slice: x: 2, y: 2, z: 4, core: 2. Of those that a mesh axis runs over, the one named last changes fastest.
Arguments:
- queries: bfloat16 [4096, 512], P('sp', 'tp'), may hold values from -6 to 6
- keys: bfloat16 [4096, 512], P('sp', 'tp'), may hold values from -6 to 6
- values: bfloat16 [4096, 512], P('sp', 'tp'), may hold values from -6 to 6
- gains: float32 [2, 128], replicated, may hold values from 0.1 to 1.9
- bias_table: float32 [192, 4], P(None, 'tp'), may hold values from -6 to 270
- d_out: bfloat16 [4096, 512], P('sp', 'tp'), may hold values from -32 to 32
Outputs:
- d_queries: bfloat16 [4096, 512], P('sp', 'tp')
- d_keys: bfloat16 [4096, 512], P('sp', 'tp')
- d_values: bfloat16 [4096, 512], P('sp', 'tp')
- d_table: float32 [192, 4], P(None, 'tp')
- d_gains: float32 [2, 128], replicated
All inputs are finite; a program needn't handle non-finite values.
Results may differ from a plain program's by a relative error of at most 0.008.
Values may be sent and summed in bfloat16 or wider, within the bound.
A program may use at most 64 MiB of HBM per device.

v0:
```python
import functools

import jax
import jax.numpy as jnp
from jax import lax
from jax.experimental import pallas as pl
from jax.experimental.pallas import tpu as pltpu
from jax.sharding import PartitionSpec as P

HEAD_DIM = 128
SEG = 64
LEFT = 4
MAX_REL = 128
EPSILON = 1e-06
NEG = -1e30
MESH = pl.DeviceIdType.MESH
F32 = jnp.float32
BF16 = jnp.bfloat16


def dot(a, b, contract, precision=None):
    return lax.dot_general(
        a, b, ((contract[:1], contract[1:]), ((), ())), preferred_element_type=F32, precision=precision
    )


def unit_of(block):
    wide = block.astype(F32)
    rms = lax.rsqrt(jnp.mean(wide * wide, axis=-1, keepdims=True) + EPSILON)
    return wide * rms, rms


def kernel(
    n_sp, n_tp,
    q_hbm, k_hbm, v_hbm, do_hbm, g_hbm, t_hbm,
    dq_ref, dk_ref, dv_ref, dt_ref, dg_ref,
    q_ref, k_ref, do_ref, g_ref, t_ref, k_raw, k_ext, v_ext, q_nxt, do_nxt, bias, bias_t, dk_acc, dv_acc,
    st_out, st_in, one_src, one, two_src, two,
    load_sem, send_sem, recv_sem, red_sem,
):
    rows, width = q_ref.shape
    heads = width // HEAD_DIM
    half = rows // 2
    window = rows + half
    entries = t_ref.shape[1]
    factor = HEAD_DIM ** (-0.5)
    sp, tp = lax.axis_index("sp"), lax.axis_index("tp")
    has_prev, has_next = sp > 0, sp < n_sp - 1

    v_ref = v_ext.at[pl.ds(rows, rows)]
    loads = [
        pltpu.make_async_copy(src, dst, load_sem.at[i])
        for i, (src, dst) in enumerate(
            [(k_hbm, k_ref), (v_hbm, v_ref), (q_hbm, q_ref), (do_hbm, do_ref), (g_hbm, g_ref), (t_hbm, t_ref)]
        )
    ]
    for load in loads:
        load.start()

    side, team = lax.rem(sp, 2), lax.div(sp, 2)
    teams = n_sp // 2

    def team_mates(action):
        for other in range(1, n_tp):
            action(sp, lax.rem(tp + other, n_tp))
        for other in range(n_tp):
            action(2 * team + 1 - side, lax.rem(tp + other, n_tp))

    def other_teams(action):
        @pl.loop(1, teams)
        def _(offset):
            at = team + offset
            at = jnp.where(at >= teams, at - teams, at)
            action(2 * at + side, tp)

    def greet(at, core):
        pl.semaphore_signal(barrier, inc=1, device_id=(at, core), device_id_type=MESH)

    barrier = pltpu.get_barrier_semaphore()
    greet(lax.rem(sp + 1, n_sp), tp)
    greet(lax.rem(sp + n_sp - 1, n_sp), tp)
    team_mates(greet)
    other_teams(greet)
    mates = 2 * n_tp - 1
    pl.semaphore_wait(barrier, 2 + mates + teams - 1)
    for load in loads:
        load.wait()

    def part(ref, index):
        return ref.at[pl.ds(index * half, half)]

    def send(slot, src, dst, to):
        return pltpu.make_async_remote_copy(
            src_ref=src, dst_ref=dst, send_sem=send_sem.at[slot], recv_sem=recv_sem.at[slot],
            device_id=(to, tp), device_id_type=MESH,
        )

    nxt, prv = sp + 1, sp - 1
    forward = [
        send(0, part(k_ref, 1), part(k_raw, 1), nxt),
        send(1, part(v_ref, 1), part(v_ext, 1), nxt),
        send(2, part(k_ref, 0), part(k_raw, 0), nxt),
        send(3, part(v_ref, 0), part(v_ext, 0), nxt),
    ]
    back = [
        send(4, part(q_ref, 0), part(q_nxt, 0), prv),
        send(5, part(do_ref, 0), part(do_nxt, 0), prv),
        send(6, part(q_ref, 1), part(q_nxt, 1), prv),
        send(7, part(do_ref, 1), part(do_nxt, 1), prv),
    ]
    stats = [send(8 + i, st_out.at[i], st_in.at[i], prv) for i in range(2)]

    def advance(done, started, gate=has_next):
        if done:
            @pl.when(has_next)
            def _():
                for copy in done:
                    copy.wait_send()

        @pl.when(gate)
        def _():
            for copy in started:
                copy.start()

    advance([], forward[:2])

    @pl.when(jnp.logical_not(has_prev))
    def _():
        k_ext[0:rows, :] = jnp.zeros((rows, width), BF16)
        v_ext[0:rows, :] = jnp.zeros((rows, width), BF16)

    head = [slice(h * HEAD_DIM, (h + 1) * HEAD_DIM) for h in range(heads)]
    g0, g1 = g_ref[0:1, :], g_ref[1:2, :]

    row = lax.broadcasted_iota(jnp.int32, (half, rows), 0)
    col = lax.broadcasted_iota(jnp.int32, (half, rows), 1)
    flip = (
        lax.broadcasted_iota(jnp.int32, (entries, rows), 0)
        + lax.broadcasted_iota(jnp.int32, (entries, rows), 1)
        == entries - 1
    ).astype(F32)
    base = dot(t_ref[...], flip, (1, 0), lax.Precision.HIGHEST)
    for h in range(heads):
        far = base[h : h + 1, 0:1]
        near = pltpu.roll(
            jnp.broadcast_to(base[h : h + 1, :], (half, rows)), 0, 1, stride=1, stride_axis=0
        )
        near = jnp.where(col <= row, far, near)
        near = jnp.where((col >= rows - SEG) & (row < SEG), NEG, near)
        first = jnp.where((col < SEG) & (row >= SEG), NEG, jnp.broadcast_to(far, (half, rows)))
        bias[h, :, 0:half] = first[:, 0:half]
        bias[h, :, half:] = near
        bias_t[h, 0:half, :] = first[:, 0:half].T
        bias_t[h, half:, :] = near[:, 0:half].T

    for h in range(heads):
        k_ext[rows:, head[h]] = (unit_of(k_ref[:, head[h]])[0] * g1).astype(BF16)

    advance(forward[:2], forward[2:])
    lane = lax.broadcasted_iota(jnp.int32, (half, HEAD_DIM), 1)
    window_col = lax.broadcasted_iota(jnp.int32, (1, window), 1)
    d_band = [None] * heads
    gain_q = jnp.zeros((1, HEAD_DIM), F32)
    gain_k = jnp.zeros((1, HEAD_DIM), F32)
    for pair in (1, 0):
        @pl.when(has_prev)
        def _():
            forward[2 * (1 - pair)].wait_recv()
            for h in range(heads):
                block = k_raw[pair * half : (pair + 1) * half, head[h]]
                k_ext[pair * half : (pair + 1) * half, head[h]] = (unit_of(block)[0] * g1).astype(BF16)
            forward[2 * (1 - pair) + 1].wait_recv()

        if pair == 0:
            advance(forward[2:], back[:2], has_prev)
        own = slice(pair * half, (pair + 1) * half)
        span = slice(pair * half, pair * half + window)
        before = rows - pair * half
        absent = jnp.where((window_col < before) & jnp.logical_not(has_prev), NEG, 0.0)
        table = jnp.zeros((half, HEAD_DIM), F32)
        for h in range(heads):
            unit, rms = unit_of(q_ref[own, head[h]])
            q_norm = (unit * g0).astype(BF16)
            d_o = do_ref[own, head[h]]
            k_win, v_win = k_ext[span, head[h]], v_ext[span, head[h]]
            scores = dot(q_norm, k_win, (1, 1)) * factor + bias[h] + absent
            top = jnp.max(scores, axis=-1, keepdims=True)
            e = jnp.exp(scores - top)
            denom = jnp.sum(e, axis=-1, keepdims=True)
            prob = e * (1.0 / denom)
            d_prob = dot(d_o, v_win, (1, 1))
            delta = jnp.sum(prob * d_prob, axis=-1, keepdims=True)
            d_score = prob * (d_prob - delta)
            table = jnp.where(lane == 2 * h, top + jnp.log(denom), table)
            table = jnp.where(lane == 2 * h + 1, delta, table)
            prob_low, d_low = prob.astype(BF16), d_score.astype(BF16)
            d_qn = dot(d_low, k_win, (1, 0)) * factor
            d_v = dot(prob_low[:, before:], d_o, (0, 0))
            d_k = dot(d_low[:, before:], q_norm, (0, 0))
            if pair == 1:
                dk_acc[:, head[h]] = d_k
                dv_acc[:, head[h]] = d_v
                d_band[h] = d_score
            else:
                dk_acc[0:half, head[h]] += d_k
                dv_acc[0:half, head[h]] += d_v
                d_band[h] = d_band[h] + d_score
            grad = d_qn * g0
            out = rms * (grad - unit * jnp.mean(grad * unit, axis=-1, keepdims=True))
            dq_ref[own, head[h]] = out.astype(BF16)
            gain_q += jnp.sum(d_qn * unit, axis=0, keepdims=True)
            gain_k += jnp.sum(d_qn * q_norm.astype(F32), axis=0, keepdims=True)
        st_out[pair] = table.T[0:8, :]

        @pl.when(has_prev)
        def _():
            stats[pair].start()

    lines = []
    for h in range(heads):
        near = d_band[h][:, half:]
        near_part = jnp.where(col > row, near, 0.0)
        far_sum = jnp.sum(d_band[h][:, 0:half] + (near - near_part)[:, 0:half], keepdims=True)
        step = half // 2
        while step:
            near_part = near_part[0:step] + pltpu.roll(near_part[step : 2 * step], rows - step, 1)
            step //= 2
        near_part = jnp.where(col[0:1] == 0, far_sum, near_part)
        lines += [near_part[:, 0:half], near_part[:, half:]]
    lines += [gain_q, gain_k]
    lines += [jnp.zeros((8 - len(lines), HEAD_DIM), F32)]
    packed = jnp.concatenate(lines, axis=0)
    one_src[...] = packed
    place = side * n_tp + tp
    one[place] = packed
    team_mates(
        lambda at, core: pltpu.make_async_remote_copy(
            src_ref=one_src, dst_ref=one.at[place], send_sem=red_sem.at[0], recv_sem=red_sem.at[1],
            device_id=(at, core), device_id_type=MESH,
        ).start()
    )
    advance([], back[2:], has_prev)
    near_peers = one.at[pl.ds(0, mates)]
    pltpu.make_async_copy(near_peers, near_peers, red_sem.at[1]).wait()
    whole = jnp.sum(one[...], axis=0)
    same = one[tp] + one[n_tp + tp]
    line = lax.broadcasted_iota(jnp.int32, whole.shape, 0)
    joined = jnp.where(line < 2 * heads, same, whole)
    two_src[...] = joined
    two[team] = joined
    other_teams(
        lambda at, core: pltpu.make_async_remote_copy(
            src_ref=two_src, dst_ref=two.at[team], send_sem=red_sem.at[2], recv_sem=red_sem.at[3],
            device_id=(at, core), device_id_type=MESH,
        ).start()
    )

    @pl.when(has_next)
    def _():
        for pair in (0, 1):
            own = slice(pair * half, rows)
            src = slice(pair * half, (pair + 1) * half)
            count = rows - pair * half
            back[2 * pair].wait_recv()
            back[2 * pair + 1].wait_recv()
            stats[pair].wait_recv()
            for h in range(heads):
                q_norm = (unit_of(q_nxt[src, head[h]])[0] * g0).astype(BF16)
                d_o = do_nxt[src, head[h]]
                k_own = k_ext[rows + pair * half : 2 * rows, head[h]]
                v_own = v_ext[rows + pair * half : 2 * rows, head[h]]
                scores = dot(k_own, q_norm, (1, 1)) * factor + bias_t[h, 0:count, :]
                prob = jnp.exp(scores - st_in[pair, 2 * h : 2 * h + 1, :])
                d_prob = dot(v_own, d_o, (1, 1))
                d_score = prob * (d_prob - st_in[pair, 2 * h + 1 : 2 * h + 2, :])
                dv_acc[own, head[h]] += dot(prob.astype(BF16), d_o, (1, 0))
                dk_acc[own, head[h]] += dot(d_score.astype(BF16), q_norm, (1, 0))

    dv_ref[...] = dv_acc[...].astype(BF16)
    for h in range(heads):
        unit, rms = unit_of(k_ref[:, head[h]])
        grad = dk_acc[:, head[h]] * factor * g1
        out = rms * (grad - unit * jnp.mean(grad * unit, axis=-1, keepdims=True))
        dk_ref[:, head[h]] = out.astype(BF16)

    far_peers = two.at[pl.ds(0, teams - 1)]
    pltpu.make_async_copy(far_peers, far_peers, red_sem.at[3]).wait()
    mine = jnp.sum(two[...], axis=0)
    band = jnp.concatenate(
        [
            jnp.concatenate([mine[2 * h : 2 * h + 1], mine[2 * h + 1 : 2 * h + 2]], axis=1)
            for h in range(heads)
        ],
        axis=0,
    )
    dt_ref[...] = dot(band, flip, (1, 1), lax.Precision.HIGHEST)
    dg_ref[0:1, :] = mine[2 * heads : 2 * heads + 1]
    dg_ref[1:2, :] = mine[2 * heads + 1 : 2 * heads + 2] / g1

    pltpu.make_async_copy(near_peers, near_peers, red_sem.at[0]).wait()
    pltpu.make_async_copy(far_peers, far_peers, red_sem.at[2]).wait()

    @pl.when(has_prev)
    def _():
        for copy in back + stats:
            copy.wait_send()


def emit(*refs):
    sem = refs[-1]
    count = len(refs) // 2
    copies = [pltpu.make_async_copy(refs[i], refs[count + i], sem.at[i]) for i in range(count)]
    for copy in copies:
        copy.start()
    for copy in copies:
        copy.wait()


def solution(mesh):
    n_sp, n_tp = mesh.shape["sp"], mesh.shape["tp"]

    def local(queries, keys, values, gains, bias_table, d_out):
        rows, width = queries.shape
        heads = width // HEAD_DIM
        assert n_sp % 2 == 0 and n_sp > 2 and rows == LEFT * SEG and 2 * heads + 2 <= 8
        act = jax.ShapeDtypeStruct((rows, width), BF16)
        half = rows // 2
        vmem = pl.BlockSpec(memory_space=pltpu.VMEM)
        shapes = (
            act, act, act,
            jax.ShapeDtypeStruct(bias_table.shape[::-1], F32),
            jax.ShapeDtypeStruct(gains.shape, F32),
        )
        parts = pl.pallas_call(
            functools.partial(kernel, n_sp, n_tp),
            out_shape=shapes,
            in_specs=[pl.BlockSpec(memory_space=pltpu.HBM)] * 6,
            out_specs=(vmem,) * 5,
            scratch_shapes=[
                pltpu.VMEM((rows, width), BF16),
                pltpu.VMEM((rows, width), BF16),
                pltpu.VMEM((rows, width), BF16),
                pltpu.VMEM(gains.shape, F32),
                pltpu.VMEM(bias_table.shape[::-1], F32),
                pltpu.VMEM((rows, width), BF16),
                pltpu.VMEM((2 * rows, width), BF16),
                pltpu.VMEM((2 * rows, width), BF16),
                pltpu.VMEM((rows, width), BF16),
                pltpu.VMEM((rows, width), BF16),
                pltpu.VMEM((heads, half, rows + half), F32),
                pltpu.VMEM((heads, rows, half), F32),
                pltpu.VMEM((rows, width), F32),
                pltpu.VMEM((rows, width), F32),
                pltpu.VMEM((2, 8, half), F32),
                pltpu.VMEM((2, 8, half), F32),
                pltpu.VMEM((8, HEAD_DIM), F32),
                pltpu.VMEM((2 * n_tp, 8, HEAD_DIM), F32),
                pltpu.VMEM((8, HEAD_DIM), F32),
                pltpu.VMEM((n_sp // 2, 8, HEAD_DIM), F32),
                pltpu.SemaphoreType.DMA((6,)),
                pltpu.SemaphoreType.DMA((10,)),
                pltpu.SemaphoreType.DMA((10,)),
                pltpu.SemaphoreType.DMA((4,)),
            ],
            compiler_params=pltpu.CompilerParams(
                collective_id=0, has_side_effects=True, vmem_limit_bytes=16 * 1024 * 1024
            ),
        )(*(
            pltpu.with_memory_space_constraint(x, pltpu.HBM)
            for x in (queries, keys, values, d_out, gains, bias_table.T)
        ))
        d_q, d_k, d_v, d_table, d_gains = pl.pallas_call(
            emit,
            out_shape=shapes,
            in_specs=[vmem] * 5,
            out_specs=(pl.BlockSpec(memory_space=pltpu.HBM),) * 5,
            scratch_shapes=[pltpu.SemaphoreType.DMA((5,))],
            compiler_params=pltpu.CompilerParams(vmem_limit_bytes=8 * 1024 * 1024),
        )(*parts)
        return d_q, d_k, d_v, d_table.T, d_gains

    in_specs = (P("sp", "tp"), P("sp", "tp"), P("sp", "tp"), P(), P(None, "tp"), P("sp", "tp"))
    out_specs = (P("sp", "tp"), P("sp", "tp"), P("sp", "tp"), P(None, "tp"), P())
    return jax.shard_map(local, mesh=mesh, in_specs=in_specs, out_specs=out_specs, check_vma=False)
```

profile of v0, /device:TPU:0, one launch (start us, length us, event | category | flops | bytes accessed | tf_op | source)
XLA Modules:
  0.0 24.3 jit_solution(17671308492289698822)
XLA Ops:
  0.6 22.9 %shard_map.101 = (bf16[256,256]{1,0:T(8,128)(2,1)S(1)}, bf16[256,256]{1,0:T(8,128)(2,1)S(1)}, bf16[256,256]{1,0:T(8,128)(2,1)S(1)}, f32[2,192]{1,0:T(2,128)S(1)}, f32[2,128]{1,0:T(2,128)S(1)}) custom-call(bf16[256,256]{1,0:T(8,128)(2,1)} %q_hbm.1, bf16[256,256]{1,0:T(8,128)(2,1)} %k_hbm.1, bf16[256,256]{1,0:T(8,128)(2,1)} %v_hbm.1, bf16[256,256]{1,0:T(8,128)(2,1)} %do_hbm.1, ...), custom_call_target="tpu_custom_call" | custom-call | tf_op jit(solution)/shard_map/pallas_call | solution.py:334
  23.5 0.8 %shard_map.102 = (bf16[256,256]{1,0:T(8,128)(2,1)}, bf16[256,256]{1,0:T(8,128)(2,1)}, bf16[256,256]{1,0:T(8,128)(2,1)}, f32[2,192]{1,0:T(2,128)}, f32[2,128]{1,0:T(2,128)}) custom-call(bf16[256,256]{1,0:T(8,128)(2,1)S(1)} %get-tuple-element.15.refs_0_, bf16[256,256]{1,0:T(8,128)(2,1)S(1)} %get-tuple-element.16.refs_1_, ...), custom_call_target="tpu_custom_call" | custom-call | tf_op jit(solution)/shard_map/pallas_call | solution.py:372
where the time goes:
time: 24.5 us; the launch traced here: 24.3 us
  Pallas kernels  23.7 us (97%)
  between operations  0.64 us (3%)
    pallas_call x1, Pallas kernels, local(): pl.pallas_call(functools.partial(kernel, n_sp, n_tp), out_shape=shapes, i...  22.9 us
    pallas_call x1, Pallas kernels, local(): pl.pallas_call(emit, out_shape=shapes, in_specs=[vmem] * 5, out_specs=(pl...  0.79 us

commit v1 on v0

v1 whole, which is shorter than its diff:
```python
import functools

import jax
import jax.numpy as jnp
from jax import lax
from jax.experimental import pallas as pl
from jax.experimental.pallas import tpu as pltpu
from jax.sharding import PartitionSpec as P

HEAD_DIM = 128
SEG = 64
LEFT = 4
MAX_REL = 128
EPSILON = 1e-06
NEG = -1e30
LOG2E = 1.4426950408889634
MESH = pl.DeviceIdType.MESH
F32 = jnp.float32
BF16 = jnp.bfloat16


def dot(a, b, contract):
    return lax.dot_general(a, b, ((contract[:1], contract[1:]), ((), ())), preferred_element_type=F32)


def unit_of(block):
    wide = block.astype(F32)
    rms = lax.rsqrt(jnp.mean(wide * wide, axis=-1, keepdims=True) + EPSILON)
    return wide * rms, rms


def diagonals(tile, lead):
    rows, lanes = tile.shape
    total = None
    for start in range(0, rows, 8):
        turned = pltpu.roll(tile[start : start + 8], (lead - start) % lanes, 1)
        total = turned if total is None else total + turned
    sublane = lax.broadcasted_iota(jnp.int32, total.shape, 0)
    line = jnp.where(sublane == 0, total, 0.0)
    for i in range(1, 8):
        line = line + jnp.where(sublane == i, pltpu.roll(total, lanes - i, 1), 0.0)
    return jnp.sum(line, axis=0, keepdims=True)


def kernel(
    n_sp, n_tp,
    q_hbm, k_hbm, v_hbm, do_hbm, g_hbm, t_hbm,
    dq_ref, dk_ref, dv_ref, dt_ref, dg_ref,
    q_ref, k_ref, v_ref, do_ref, g_ref, t_ref, k_raw, v_prev, kn, qn, q_unit, q_rms, k_unit, k_rms,
    tiles, e_own, dp_own, dk_acc, dv_acc, dk_out, dv_out, dk_in, dv_in, one_src, two, line_src, lines,
    load_sem, send_sem, recv_sem, red_sem, hand_sem,
):
    heads, rows, _ = q_ref.shape
    half = rows // 2
    entries = t_ref.shape[1]
    lead = SEG - 1
    factor = HEAD_DIM ** (-0.5)
    scale = factor * LOG2E
    sp, tp = lax.axis_index("sp"), lax.axis_index("tp")
    has_prev, has_next = sp > 0, sp < n_sp - 1
    nxt, prv = sp + 1, sp - 1

    def load(src, dst, slot):
        return pltpu.make_async_copy(src, dst, load_sem.at[slot])

    def by_head(src, dst, slot):
        return [load(src.at[:, pl.ds(h * HEAD_DIM, HEAD_DIM)], dst.at[h], slot + h) for h in range(heads)]

    load_k = by_head(k_hbm, k_ref, 0)
    load_v = by_head(v_hbm, v_ref, heads)
    load_small = [load(t_hbm, t_ref, 4 * heads), load(g_hbm, g_ref, 4 * heads + 1)]
    load_q = by_head(q_hbm, q_ref, 2 * heads)
    load_do = by_head(do_hbm, do_ref, 3 * heads)
    for copy in load_k + load_v + load_small + load_q + load_do:
        copy.start()

    def signal(sem, at, core):
        pl.semaphore_signal(sem, inc=1, device_id=(at, core), device_id_type=MESH)

    def around(sem, radius):
        @pl.when(sp >= radius)
        def _():
            signal(sem, sp - radius, tp)

        @pl.when(sp < n_sp - radius)
        def _():
            signal(sem, sp + radius, tp)

    def count_around(radius):
        return jnp.where(sp >= radius, 1, 0) + jnp.where(sp < n_sp - radius, 1, 0)

    barrier = pltpu.get_barrier_semaphore()
    around(barrier, 1)
    for other in range(1, n_tp):
        signal(barrier, sp, lax.rem(tp + other, n_tp))
    pl.semaphore_wait(barrier, count_around(1) + n_tp - 1)

    rounds = []
    while 2 ** len(rounds) < n_sp:
        rounds.append(2 ** len(rounds))

    def say(step):
        around(hand_sem.at[step], rounds[step])

    def hear(step):
        pl.semaphore_wait(hand_sem.at[step], count_around(rounds[step]))

    def send(slot, src, dst, to):
        return pltpu.make_async_remote_copy(
            src_ref=src, dst_ref=dst, send_sem=send_sem.at[slot], recv_sem=recv_sem.at[slot],
            device_id=(to, tp), device_id_type=MESH,
        )

    k_next = [send(4 * h, k_ref.at[h], k_raw.at[h], nxt) for h in range(heads)]
    v_next = [send(4 * h + 1, v_ref.at[h], v_prev.at[h], nxt) for h in range(heads)]
    dv_back = [send(4 * h + 2, dv_out.at[h], dv_in.at[h], prv) for h in range(heads)]
    dk_back = [send(4 * h + 3, dk_out.at[h], dk_in.at[h], prv) for h in range(heads)]

    def start(gate, copies):
        @pl.when(gate)
        def _():
            for copy in copies:
                copy.start()

    for copy in load_k + load_v:
        copy.wait()
    for h in range(heads):
        start(has_next, [k_next[h], v_next[h]])
    say(0)
    for copy in load_small:
        copy.wait()

    @pl.when(jnp.logical_not(has_prev))
    def _():
        kn[:, 0:rows, :] = jnp.zeros((heads, rows, HEAD_DIM), BF16)
        v_prev[...] = jnp.zeros((heads, rows, HEAD_DIM), BF16)

    g0, g1 = g_ref[0:1, :], g_ref[1:2, :]
    low, high = slice(0, half), slice(half, rows)
    row = lax.broadcasted_iota(jnp.int32, (half, half), 0)
    col = lax.broadcasted_iota(jnp.int32, (half, half), 1)
    upper = col >= row
    absent = jnp.where(has_prev, 0.0, NEG)

    table = jnp.concatenate([t_ref[...], jnp.zeros((heads, 2 * half - entries), F32)], axis=1)
    table = pltpu.roll(table, 2 * half - lead, 1)
    for h in range(heads):
        def skew(line):
            return pltpu.roll(jnp.broadcast_to(line, (half, half)), 0, 1, stride=1, stride_axis=0)

        near = skew(table[h : h + 1, 0:half])
        ahead = skew(table[h : h + 1, half:])
        far = jnp.broadcast_to(table[h : h + 1, half : half + 1], (half, half))
        same = jnp.where(upper, near, ahead)
        same = jnp.where((row >= SEG) & (col < SEG), NEG, same)
        before = jnp.where(upper, far, near)
        distant = jnp.where((row < SEG) & (col >= SEG), NEG, far)
        top_own = jnp.max(same, axis=0, keepdims=True)
        top = jnp.maximum(top_own, jnp.max(before, axis=0, keepdims=True))
        first_top = jnp.where(has_prev, top, top_own)
        tiles[h, 0] = (same - first_top) * LOG2E
        tiles[h, 1] = (before - top) * LOG2E
        tiles[h, 2] = (same - top) * LOG2E
        tiles[h, 3] = (distant - top) * LOG2E + absent
        tiles[h, 4] = (before - top) * LOG2E + absent

    for h in range(heads):
        unit, rms = unit_of(k_ref[h])
        k_unit[h] = unit
        k_rms[h] = rms
        kn[h, rows:, :] = (unit * g1).astype(BF16)
    hear(0)
    say(1)
    for copy in load_q + load_do:
        copy.wait()

    sums = []
    for h in range(heads):
        unit, rms = unit_of(q_ref[h])
        q_unit[h] = unit
        q_rms[h] = rms
        qn[h] = (unit * g0).astype(BF16)
        s0 = dot(kn[h, rows : rows + half, :], qn[h], (1, 1)) * scale
        s1 = dot(kn[h, rows + half :, :], qn[h, high, :], (1, 1)) * scale
        e0 = jnp.exp2(s0[:, low] + tiles[h, 0])
        e1 = jnp.exp2(s0[:, high] + tiles[h, 1])
        e2 = jnp.exp2(s1 + tiles[h, 2])
        e_own[h, 0], e_own[h, 1], e_own[h, 2] = e0, e1, e2
        p0 = dot(v_ref[h, low, :], do_ref[h], (1, 1))
        dp_own[h, 0], dp_own[h, 1] = p0[:, low], p0[:, high]
        dp_own[h, 2] = dot(v_ref[h, high, :], do_ref[h, high, :], (1, 1))
        sums.append((
            jnp.sum(e0, axis=0, keepdims=True),
            jnp.sum(e1, axis=0, keepdims=True) + jnp.sum(e2, axis=0, keepdims=True),
        ))
        if h + 1 < len(rounds):
            hear(h + 1)
        if h + 2 < len(rounds):
            say(h + 2)
    for step in range(heads + 1, len(rounds)):
        hear(step)
        if step + 1 < len(rounds):
            say(step + 1)

    packed = []
    mass = jnp.zeros((1, HEAD_DIM), F32)
    for h in range(heads):
        @pl.when(has_prev)
        def _():
            k_next[h].wait_recv()
            kn[h, 0:rows, :] = (unit_of(k_raw[h])[0] * g1).astype(BF16)

        s0 = dot(kn[h, low, :], qn[h, low, :], (1, 1)) * scale
        s1 = dot(kn[h, high, :], qn[h], (1, 1)) * scale
        x0 = jnp.exp2(s0 + tiles[h, 3])
        x1 = jnp.exp2(s1[:, low] + tiles[h, 4])
        x2 = jnp.exp2(s1[:, high] + tiles[h, 3])
        r0 = 1.0 / (sums[h][0] + jnp.sum(x0 + x1, axis=0, keepdims=True))
        r1 = 1.0 / (sums[h][1] + jnp.sum(x2, axis=0, keepdims=True))
        x0, x1, x2 = x0 * r0, x1 * r0, x2 * r1
        e0, e1, e2 = e_own[h, 0] * r0, e_own[h, 1] * r1, e_own[h, 2] * r1
        d_o = do_ref[h]
        dv_out[h, low, :] = dot(x0.astype(BF16), d_o[low], (1, 0)).astype(BF16)
        dv_out[h, high, :] = dot(jnp.concatenate([x1, x2], axis=1).astype(BF16), d_o, (1, 0)).astype(BF16)
        dv_acc[h, low, :] = dot(jnp.concatenate([e0, e1], axis=1).astype(BF16), d_o, (1, 0))
        dv_acc[h, high, :] = dot(e2.astype(BF16), d_o[high], (1, 0))
        if h < heads - 1:
            start(has_prev, [dv_back[h]])
        own0 = jnp.sum(e0 * dp_own[h, 0], axis=0, keepdims=True)
        own1 = jnp.sum(e1 * dp_own[h, 1] + e2 * dp_own[h, 2], axis=0, keepdims=True)

        @pl.when(has_prev)
        def _():
            v_next[h].wait_recv()

        p0 = dot(v_prev[h, low, :], d_o[low], (1, 1))
        p1 = dot(v_prev[h, high, :], d_o, (1, 1))
        delta0 = own0 + jnp.sum(x0 * p0 + x1 * p1[:, low], axis=0, keepdims=True)
        delta1 = own1 + jnp.sum(x2 * p1[:, high], axis=0, keepdims=True)
        x0, x1, x2 = x0 * (p0 - delta0), x1 * (p1[:, low] - delta0), x2 * (p1[:, high] - delta1)
        e0, e1, e2 = e0 * (dp_own[h, 0] - delta0), e1 * (dp_own[h, 1] - delta1), e2 * (dp_own[h, 2] - delta1)
        blocks = [
            x0.astype(BF16),
            jnp.concatenate([x1, x2], axis=1).astype(BF16),
            jnp.concatenate([e0, e1], axis=1).astype(BF16),
            e2.astype(BF16),
        ]
        spans = [low, slice(0, rows), slice(0, rows), high]
        d_k = [dot(block, qn[h, span, :], (1, 0)) for block, span in zip(blocks, spans)]
        product = None
        for i, part in enumerate(d_k):
            term = part * kn[h, i * half : (i + 1) * half, :].astype(F32)
            product = term if product is None else product + term
        mass = mass + jnp.sum(product, axis=0, keepdims=True)
        same, before = e0 + e2, x1 + e1
        line_p = diagonals(jnp.where(upper, same, before), lead)
        line_n = diagonals(jnp.where(upper, 0.0, same), lead)
        lane = lax.broadcasted_iota(jnp.int32, line_p.shape, 1)
        rest = -(jnp.sum(line_p, axis=1, keepdims=True) + jnp.sum(line_n, axis=1, keepdims=True))
        packed.append(jnp.where(lane < lead, line_n, line_p))
        packed.append(jnp.where(lane < lead, line_p, jnp.where(lane == lead, rest, 0.0)))
        dk_out[h, low, :] = d_k[0].astype(BF16)
        dk_out[h, high, :] = d_k[1].astype(BF16)
        dk_acc[h, low, :] = d_k[2]
        dk_acc[h, high, :] = d_k[3]
        if h < heads - 1:
            start(has_prev, [dk_back[h]])
        else:
            mass = mass * factor
            line_src[...] = mass
            one_src[...] = jnp.concatenate(
                packed + [mass, jnp.zeros((8 - 1 - len(packed), HEAD_DIM), F32)], axis=0
            )
            two[sp] = one_src[...]

            def spread(i):
                at = jnp.where(i >= sp, i + 1, i)
                pltpu.make_async_remote_copy(
                    src_ref=one_src, dst_ref=two.at[sp], send_sem=red_sem.at[0], recv_sem=red_sem.at[1],
                    device_id=(at, tp), device_id_type=MESH,
                ).start()

            def spread_line(at):
                for other in range(1, n_tp):
                    pltpu.make_async_remote_copy(
                        src_ref=line_src, dst_ref=lines.at[other - 1, sp], send_sem=red_sem.at[2],
                        recv_sem=red_sem.at[3], device_id=(at, lax.rem(tp + other, n_tp)), device_id_type=MESH,
                    ).start()

            if n_sp <= 32:
                for i in range(n_sp - 1):
                    spread(i)
                    spread_line(i)
                spread_line(n_sp - 1)
            else:
                @pl.loop(0, n_sp - 1)
                def _(i):
                    spread(i)

                @pl.loop(0, n_sp)
                def _(i):
                    spread_line(i)

            start(has_prev, [dv_back[h], dk_back[h]])
        for i, part in enumerate([
            dot(jnp.concatenate([blocks[0], blocks[1][:, low], blocks[2][:, low]], axis=0), kn[h, 0 : 3 * half, :], (0, 0)),
            dot(jnp.concatenate([blocks[1][:, high], blocks[2][:, high], blocks[3]], axis=0), kn[h, half:, :], (0, 0)),
        ]):
            span = slice(i * half, (i + 1) * half)
            grad = part * factor * g0
            unit = q_unit[h, span, :]
            out = q_rms[h, span, :] * (grad - unit * jnp.mean(grad * unit, axis=-1, keepdims=True))
            dq_ref[span, h * HEAD_DIM : (h + 1) * HEAD_DIM] = out.astype(BF16)

    for h in range(heads):
        across = slice(h * HEAD_DIM, (h + 1) * HEAD_DIM)

        @pl.when(has_next)
        def _():
            dv_back[h].wait_recv()
            dk_back[h].wait_recv()
            dv_acc[h] += dv_in[h].astype(F32)
            dk_acc[h] += dk_in[h].astype(F32)

        dv_ref[:, across] = dv_acc[h].astype(BF16)
        unit = k_unit[h]
        grad = dk_acc[h] * factor * g1
        out = k_rms[h] * (grad - unit * jnp.mean(grad * unit, axis=-1, keepdims=True))
        dk_ref[:, across] = out.astype(BF16)

    inverse = 1.0 / g_ref[...]
    peers = two.at[pl.ds(0, n_sp - 1)]
    pltpu.make_async_copy(peers, peers, red_sem.at[1]).wait()
    pltpu.make_async_copy(lines, lines, red_sem.at[3]).wait()
    whole = jnp.sum(two[...], axis=0)
    for h in range(heads):
        dt_ref[h : h + 1, 0:half] = whole[2 * h : 2 * h + 1]
        dt_ref[h : h + 1, half:] = whole[2 * h + 1 : 2 * h + 2, 0 : entries - half]
    mass = whole[2 * heads : 2 * heads + 1] + jnp.sum(lines[...], axis=(0, 1))
    dg_ref[...] = mass * inverse

    pltpu.make_async_copy(peers, peers, red_sem.at[0]).wait()
    pltpu.make_async_copy(lines, lines, red_sem.at[2]).wait()

    @pl.when(has_next)
    def _():
        for copy in k_next + v_next:
            copy.wait_send()

    @pl.when(has_prev)
    def _():
        for copy in dv_back + dk_back:
            copy.wait_send()


def emit(*refs):
    sem = refs[-1]
    count = len(refs) // 2
    copies = [pltpu.make_async_copy(refs[i], refs[count + i], sem.at[i]) for i in range(count)]
    for copy in copies:
        copy.start()
    for copy in copies:
        copy.wait()


def solution(mesh):
    n_sp, n_tp = mesh.shape["sp"], mesh.shape["tp"]

    def local(queries, keys, values, gains, bias_table, d_out):
        rows, width = queries.shape
        heads = width // HEAD_DIM
        half = rows // 2
        assert n_sp > 1 and rows == LEFT * SEG and half == MAX_REL == HEAD_DIM and 2 * heads + 1 <= 8
        act = jax.ShapeDtypeStruct((rows, width), BF16)
        vmem = pl.BlockSpec(memory_space=pltpu.VMEM)
        shapes = (
            act, act, act,
            jax.ShapeDtypeStruct(bias_table.shape[::-1], F32),
            jax.ShapeDtypeStruct(gains.shape, F32),
        )
        low = pltpu.VMEM((heads, rows, HEAD_DIM), BF16)
        wide = pltpu.VMEM((heads, rows, HEAD_DIM), F32)
        thin = pltpu.VMEM((heads, rows, 1), F32)
        parts = pl.pallas_call(
            functools.partial(kernel, n_sp, n_tp),
            out_shape=shapes,
            in_specs=[pl.BlockSpec(memory_space=pltpu.HBM)] * 6,
            out_specs=(vmem,) * 5,
            scratch_shapes=[
                low, low, low, low,
                pltpu.VMEM(gains.shape, F32),
                pltpu.VMEM(bias_table.shape[::-1], F32),
                low, low,
                pltpu.VMEM((heads, 2 * rows, HEAD_DIM), BF16),
                low,
                wide, thin, wide, thin,
                pltpu.VMEM((heads, 5, half, half), F32),
                pltpu.VMEM((heads, 3, half, half), F32),
                pltpu.VMEM((heads, 3, half, half), F32),
                wide, wide,
                low, low, low, low,
                pltpu.VMEM((8, HEAD_DIM), F32),
                pltpu.VMEM((n_sp, 8, HEAD_DIM), F32),
                pltpu.VMEM((1, HEAD_DIM), F32),
                pltpu.VMEM((n_tp - 1, n_sp, 1, HEAD_DIM), F32),
                pltpu.SemaphoreType.DMA((4 * heads + 2,)),
                pltpu.SemaphoreType.DMA((4 * heads,)),
                pltpu.SemaphoreType.DMA((4 * heads,)),
                pltpu.SemaphoreType.DMA((4,)),
                pltpu.SemaphoreType.REGULAR((max(1, (n_sp - 1).bit_length()),)),
            ],
            compiler_params=pltpu.CompilerParams(
                collective_id=0, has_side_effects=True, vmem_limit_bytes=24 * 1024 * 1024
            ),
        )(*(
            pltpu.with_memory_space_constraint(x, pltpu.HBM)
            for x in (queries, keys, values, d_out, gains, bias_table.T)
        ))
        d_q, d_k, d_v, d_table, d_gains = pl.pallas_call(
            emit,
            out_shape=shapes,
            in_specs=[vmem] * 5,
            out_specs=(pl.BlockSpec(memory_space=pltpu.HBM),) * 5,
            scratch_shapes=[pltpu.SemaphoreType.DMA((5,))],
            compiler_params=pltpu.CompilerParams(vmem_limit_bytes=8 * 1024 * 1024),
        )(*parts)
        return d_q, d_k, d_v, d_table.T, d_gains

    in_specs = (P("sp", "tp"), P("sp", "tp"), P("sp", "tp"), P(), P(None, "tp"), P("sp", "tp"))
    out_specs = (P("sp", "tp"), P("sp", "tp"), P("sp", "tp"), P(None, "tp"), P())
    return jax.shard_map(local, mesh=mesh, in_specs=in_specs, out_specs=out_specs, check_vma=False)
```

time: 24.5 us -> 21.1 us (0.86)
  Pallas kernels: 23.7 us -> 20.3 us
    pallas_call x1, Pallas kernels: 22.9 us -> 19.5 us  [local(): pl.pallas_call(functools.partial(kernel, n_sp, n_tp), out_shape=shapes, i...]
where the time goes in v1:
time: 21.1 us; the launch traced here: 21 us
  Pallas kernels  20.3 us (96%)
  between operations  0.64 us (3%)
    pallas_call x1, Pallas kernels, local(): pl.pallas_call(functools.partial(kernel, n_sp, n_tp), out_shape=shapes, i...  19.5 us
    pallas_call x1, Pallas kernels, local(): pl.pallas_call(emit, out_shape=shapes, in_specs=[vmem] * 5, out_specs=(pl...  0.79 us

profile of v1, /device:TPU:0, one launch (start us, length us, event | category | flops | bytes accessed | tf_op | source)
XLA Modules:
  0.0 21.0 jit_solution(1963416285211649662)
XLA Ops:
  0.6 19.5 %shard_map.101 = (bf16[256,256]{1,0:T(8,128)(2,1)S(1)}, bf16[256,256]{1,0:T(8,128)(2,1)S(1)}, bf16[256,256]{1,0:T(8,128)(2,1)S(1)}, f32[2,192]{1,0:T(2,128)S(1)}, f32[2,128]{1,0:T(2,128)S(1)}) custom-call(bf16[256,256]{1,0:T(8,128)(2,1)} %q_hbm.1, bf16[256,256]{1,0:T(8,128)(2,1)} %k_hbm.1, bf16[256,256]{1,0:T(8,128)(2,1)} %v_hbm.1, bf16[256,256]{1,0:T(8,128)(2,1)} %do_hbm.1, ...), custom_call_target="tpu_custom_call" | custom-call | tf_op jit(solution)/shard_map/pallas_call | solution.py:384
  20.2 0.8 %shard_map.102 = (bf16[256,256]{1,0:T(8,128)(2,1)}, bf16[256,256]{1,0:T(8,128)(2,1)}, bf16[256,256]{1,0:T(8,128)(2,1)}, f32[2,192]{1,0:T(2,128)}, f32[2,128]{1,0:T(2,128)}) custom-call(bf16[256,256]{1,0:T(8,128)(2,1)S(1)} %get-tuple-element.15.refs_0_, bf16[256,256]{1,0:T(8,128)(2,1)S(1)} %get-tuple-element.16.refs_1_, ...), custom_call_target="tpu_custom_call" | custom-call | tf_op jit(solution)/shard_map/pallas_call | solution.py:419

commit v2 on v1

--- a/solution.py
+++ b/solution.py
@@ -124,8 +124,9 @@
 
     for copy in load_k + load_v:
         copy.wait()
-    for h in range(heads):
-        start(has_next, [k_next[h], v_next[h]])
+    yields = tp == n_tp - 1
+    start(has_next, [k_next[0], v_next[0]])
+    start(has_next & jnp.logical_not(yields), k_next[1:] + v_next[1:])
     say(0)
     for copy in load_small:
         copy.wait()
@@ -148,12 +149,12 @@
         def skew(line):
             return pltpu.roll(jnp.broadcast_to(line, (half, half)), 0, 1, stride=1, stride_axis=0)
 
-        near = skew(table[h : h + 1, 0:half])
+        close = skew(table[h : h + 1, 0:half])
         ahead = skew(table[h : h + 1, half:])
         far = jnp.broadcast_to(table[h : h + 1, half : half + 1], (half, half))
-        same = jnp.where(upper, near, ahead)
+        same = jnp.where(upper, close, ahead)
         same = jnp.where((row >= SEG) & (col < SEG), NEG, same)
-        before = jnp.where(upper, far, near)
+        before = jnp.where(upper, far, close)
         distant = jnp.where((row < SEG) & (col >= SEG), NEG, far)
         top_own = jnp.max(same, axis=0, keepdims=True)
         top = jnp.maximum(top_own, jnp.max(before, axis=0, keepdims=True))
@@ -169,8 +170,6 @@
         k_unit[h] = unit
         k_rms[h] = rms
         kn[h, rows:, :] = (unit * g1).astype(BF16)
-    hear(0)
-    say(1)
     for copy in load_q + load_do:
         copy.wait()
 
@@ -193,15 +192,18 @@
             jnp.sum(e0, axis=0, keepdims=True),
             jnp.sum(e1, axis=0, keepdims=True) + jnp.sum(e2, axis=0, keepdims=True),
         ))
-        if h + 1 < len(rounds):
-            hear(h + 1)
-        if h + 2 < len(rounds):
-            say(h + 2)
-    for step in range(heads + 1, len(rounds)):
-        hear(step)
-        if step + 1 < len(rounds):
-            say(step + 1)
-
+    step = 0
+
+    def relay(step):
+        if step < len(rounds):
+            hear(step)
+            if step + 1 < len(rounds):
+                say(step + 1)
+        return step + 1
+
+    step = relay(step)
+    step = relay(step)
+    start(has_next & yields, k_next[1:] + v_next[1:])
     packed = []
     mass = jnp.zeros((1, HEAD_DIM), F32)
     for h in range(heads):
@@ -224,8 +226,7 @@
         dv_out[h, high, :] = dot(jnp.concatenate([x1, x2], axis=1).astype(BF16), d_o, (1, 0)).astype(BF16)
         dv_acc[h, low, :] = dot(jnp.concatenate([e0, e1], axis=1).astype(BF16), d_o, (1, 0))
         dv_acc[h, high, :] = dot(e2.astype(BF16), d_o[high], (1, 0))
-        if h < heads - 1:
-            start(has_prev, [dv_back[h]])
+        step = relay(step)
         own0 = jnp.sum(e0 * dp_own[h, 0], axis=0, keepdims=True)
         own1 = jnp.sum(e1 * dp_own[h, 1] + e2 * dp_own[h, 2], axis=0, keepdims=True)
 
@@ -264,8 +265,10 @@
         dk_acc[h, low, :] = d_k[2]
         dk_acc[h, high, :] = d_k[3]
         if h < heads - 1:
-            start(has_prev, [dk_back[h]])
+            start(has_prev, [dv_back[h], dk_back[h]])
         else:
+            while step < len(rounds):
+                step = relay(step)
             mass = mass * factor
             line_src[...] = mass
             one_src[...] = jnp.concatenate(

time: 21.1 us -> 19.6 us (0.929)
  Pallas kernels: 20.3 us -> 18.8 us
    pallas_call x1, Pallas kernels: 19.5 us -> 18 us  [local(): pl.pallas_call(functools.partial(kernel, n_sp, n_tp), out_shape=shapes, i...]
where the time goes in v2:
time: 19.6 us; the launch traced here: 19.4 us
  Pallas kernels  18.8 us (96%)
  between operations  0.64 us (3%)
    pallas_call x1, Pallas kernels, local(): pl.pallas_call(functools.partial(kernel, n_sp, n_tp), out_shape=shapes, i...  18 us
    pallas_call x1, Pallas kernels, local(): pl.pallas_call(emit, out_shape=shapes, in_specs=[vmem] * 5, out_specs=(pl...  0.79 us

profile of v2, /device:TPU:0, one launch (start us, length us, event | category | flops | bytes accessed | tf_op | source)
XLA Modules:
  0.0 19.4 jit_solution(12468274605366717738)
XLA Ops:
  0.6 18.0 %shard_map.101 = (bf16[256,256]{1,0:T(8,128)(2,1)S(1)}, bf16[256,256]{1,0:T(8,128)(2,1)S(1)}, bf16[256,256]{1,0:T(8,128)(2,1)S(1)}, f32[2,192]{1,0:T(2,128)S(1)}, f32[2,128]{1,0:T(2,128)S(1)}) custom-call(bf16[256,256]{1,0:T(8,128)(2,1)} %q_hbm.1, bf16[256,256]{1,0:T(8,128)(2,1)} %k_hbm.1, bf16[256,256]{1,0:T(8,128)(2,1)} %v_hbm.1, bf16[256,256]{1,0:T(8,128)(2,1)} %do_hbm.1, ...), custom_call_target="tpu_custom_call" | custom-call | tf_op jit(solution)/shard_map/pallas_call | solution.py:387
  18.6 0.8 %shard_map.102 = (bf16[256,256]{1,0:T(8,128)(2,1)}, bf16[256,256]{1,0:T(8,128)(2,1)}, bf16[256,256]{1,0:T(8,128)(2,1)}, f32[2,192]{1,0:T(2,128)}, f32[2,128]{1,0:T(2,128)}) custom-call(bf16[256,256]{1,0:T(8,128)(2,1)S(1)} %get-tuple-element.15.refs_0_, bf16[256,256]{1,0:T(8,128)(2,1)S(1)} %get-tuple-element.16.refs_1_, ...), custom_call_target="tpu_custom_call" | custom-call | tf_op jit(solution)/shard_map/pallas_call | solution.py:422

commit v3 on v2

--- a/solution.py
+++ b/solution.py
@@ -125,6 +125,7 @@
     for copy in load_k + load_v:
         copy.wait()
     yields = tp == n_tp - 1
+    eager = sp < n_sp // 4
     start(has_next, [k_next[0], v_next[0]])
     start(has_next & jnp.logical_not(yields), k_next[1:] + v_next[1:])
     say(0)
@@ -203,7 +204,6 @@
 
     step = relay(step)
     step = relay(step)
-    start(has_next & yields, k_next[1:] + v_next[1:])
     packed = []
     mass = jnp.zeros((1, HEAD_DIM), F32)
     for h in range(heads):
@@ -226,7 +226,12 @@
         dv_out[h, high, :] = dot(jnp.concatenate([x1, x2], axis=1).astype(BF16), d_o, (1, 0)).astype(BF16)
         dv_acc[h, low, :] = dot(jnp.concatenate([e0, e1], axis=1).astype(BF16), d_o, (1, 0))
         dv_acc[h, high, :] = dot(e2.astype(BF16), d_o[high], (1, 0))
-        step = relay(step)
+        if h == 0:
+            start(has_next & yields, k_next[1:])
+        if step < len(rounds) - 1:
+            step = relay(step)
+        if h == 0:
+            start(has_next & yields, v_next[1:])
         own0 = jnp.sum(e0 * dp_own[h, 0], axis=0, keepdims=True)
         own1 = jnp.sum(e1 * dp_own[h, 1] + e2 * dp_own[h, 2], axis=0, keepdims=True)
 
@@ -267,8 +272,6 @@
         if h < heads - 1:
             start(has_prev, [dv_back[h], dk_back[h]])
         else:
-            while step < len(rounds):
-                step = relay(step)
             mass = mass * factor
             line_src[...] = mass
             one_src[...] = jnp.concatenate(
@@ -290,21 +293,28 @@
                         recv_sem=red_sem.at[3], device_id=(at, lax.rem(tp + other, n_tp)), device_id_type=MESH,
                     ).start()
 
-            if n_sp <= 32:
-                for i in range(n_sp - 1):
-                    spread(i)
-                    spread_line(i)
-                spread_line(n_sp - 1)
-            else:
-                @pl.loop(0, n_sp - 1)
-                def _(i):
-                    spread(i)
-
-                @pl.loop(0, n_sp)
-                def _(i):
-                    spread_line(i)
-
-            start(has_prev, [dv_back[h], dk_back[h]])
+            def publish():
+                for late in range(step, len(rounds)):
+                    relay(late)
+                if n_sp <= 32:
+                    for i in range(n_sp - 1):
+                        spread(i)
+                        spread_line(i)
+                    spread_line(n_sp - 1)
+                else:
+                    @pl.loop(0, n_sp - 1)
+                    def _(i):
+                        spread(i)
+
+                    @pl.loop(0, n_sp)
+                    def _(i):
+                        spread_line(i)
+
+            @pl.when(jnp.logical_not(eager))
+            def _():
+                publish()
+
+            start(has_prev & jnp.logical_not(yields), [dk_back[h], dv_back[h]])
         for i, part in enumerate([
             dot(jnp.concatenate([blocks[0], blocks[1][:, low], blocks[2][:, low]], axis=0), kn[h, 0 : 3 * half, :], (0, 0)),
             dot(jnp.concatenate([blocks[1][:, high], blocks[2][:, high], blocks[3]], axis=0), kn[h, half:, :], (0, 0)),
@@ -315,21 +325,47 @@
             out = q_rms[h, span, :] * (grad - unit * jnp.mean(grad * unit, axis=-1, keepdims=True))
             dq_ref[span, h * HEAD_DIM : (h + 1) * HEAD_DIM] = out.astype(BF16)
 
+    @pl.when(eager)
+    def _():
+        publish()
+
+    def add_dv(h):
+        @pl.when(has_next)
+        def _():
+            dv_acc[h] += dv_in[h].astype(F32)
+
+        dv_ref[:, h * HEAD_DIM : (h + 1) * HEAD_DIM] = dv_acc[h].astype(BF16)
+
     for h in range(heads):
         across = slice(h * HEAD_DIM, (h + 1) * HEAD_DIM)
 
         @pl.when(has_next)
         def _():
-            dv_back[h].wait_recv()
-            dk_back[h].wait_recv()
-            dv_acc[h] += dv_in[h].astype(F32)
+            (dv_back if h < heads - 1 else dk_back)[h].wait_recv()
+
+        if h == 0:
+            start(has_prev & yields, [dk_back[heads - 1], dv_back[heads - 1]])
+        if h < heads - 1:
+            add_dv(h)
+
+            @pl.when(has_next)
+            def _():
+                dk_back[h].wait_recv()
+
+        @pl.when(has_next)
+        def _():
             dk_acc[h] += dk_in[h].astype(F32)
 
-        dv_ref[:, across] = dv_acc[h].astype(BF16)
         unit = k_unit[h]
         grad = dk_acc[h] * factor * g1
         out = k_rms[h] * (grad - unit * jnp.mean(grad * unit, axis=-1, keepdims=True))
         dk_ref[:, across] = out.astype(BF16)
+        if h == heads - 1:
+            @pl.when(has_next)
+            def _():
+                dv_back[h].wait_recv()
+
+            add_dv(h)
 
     inverse = 1.0 / g_ref[...]
     peers = two.at[pl.ds(0, n_sp - 1)]

time: 19.6 us -> 19.1 us (0.974)
  Pallas kernels: 18.8 us -> 18.1 us
    pallas_call x1, Pallas kernels: 18 us -> 17.4 us  [local(): pl.pallas_call(functools.partial(kernel, n_sp, n_tp), out_shape=shapes, i...]
where the time goes in v3:
time: 19.1 us; the launch traced here: 18.8 us
  Pallas kernels  18.1 us (95%)
  between operations  0.64 us (3%)
    pallas_call x1, Pallas kernels, local(): pl.pallas_call(functools.partial(kernel, n_sp, n_tp), out_shape=shapes, i...  17.4 us
    pallas_call x1, Pallas kernels, local(): pl.pallas_call(emit, out_shape=shapes, in_specs=[vmem] * 5, out_specs=(pl...  0.79 us

profile of v3, /device:TPU:0, one launch (start us, length us, event | category | flops | bytes accessed | tf_op | source)
XLA Modules:
  0.0 18.8 jit_solution(14364671214325720297)
XLA Ops:
  0.6 17.4 %shard_map.101 = (bf16[256,256]{1,0:T(8,128)(2,1)S(1)}, bf16[256,256]{1,0:T(8,128)(2,1)S(1)}, bf16[256,256]{1,0:T(8,128)(2,1)S(1)}, f32[2,192]{1,0:T(2,128)S(1)}, f32[2,128]{1,0:T(2,128)S(1)}) custom-call(bf16[256,256]{1,0:T(8,128)(2,1)} %q_hbm.1, bf16[256,256]{1,0:T(8,128)(2,1)} %k_hbm.1, bf16[256,256]{1,0:T(8,128)(2,1)} %v_hbm.1, bf16[256,256]{1,0:T(8,128)(2,1)} %do_hbm.1, ...), custom_call_target="tpu_custom_call" | custom-call | tf_op jit(solution)/shard_map/pallas_call | solution.py:423
  18.0 0.8 %shard_map.102 = (bf16[256,256]{1,0:T(8,128)(2,1)}, bf16[256,256]{1,0:T(8,128)(2,1)}, bf16[256,256]{1,0:T(8,128)(2,1)}, f32[2,192]{1,0:T(2,128)}, f32[2,128]{1,0:T(2,128)}) custom-call(bf16[256,256]{1,0:T(8,128)(2,1)S(1)} %get-tuple-element.15.refs_0_, bf16[256,256]{1,0:T(8,128)(2,1)S(1)} %get-tuple-element.16.refs_1_, ...), custom_call_target="tpu_custom_call" | custom-call | tf_op jit(solution)/shard_map/pallas_call | solution.py:458

commit v4 on v3

--- a/solution.py
+++ b/solution.py
@@ -29,12 +29,16 @@
     return wide * rms, rms
 
 
-def diagonals(tile, lead):
-    rows, lanes = tile.shape
+def fold(tile, lead):
     total = None
-    for start in range(0, rows, 8):
-        turned = pltpu.roll(tile[start : start + 8], (lead - start) % lanes, 1)
+    for start in range(0, tile.shape[0], 8):
+        turned = pltpu.roll(tile[start : start + 8], (lead - start) % tile.shape[1], 1)
         total = turned if total is None else total + turned
+    return total
+
+
+def align(total):
+    lanes = total.shape[1]
     sublane = lax.broadcasted_iota(jnp.int32, total.shape, 0)
     line = jnp.where(sublane == 0, total, 0.0)
     for i in range(1, 8):
@@ -46,11 +50,14 @@
     n_sp, n_tp,
     q_hbm, k_hbm, v_hbm, do_hbm, g_hbm, t_hbm,
     dq_ref, dk_ref, dv_ref, dt_ref, dg_ref,
-    q_ref, k_ref, v_ref, do_ref, g_ref, t_ref, k_raw, v_prev, kn, qn, q_unit, q_rms, k_unit, k_rms,
-    tiles, e_own, dp_own, dk_acc, dv_acc, dk_out, dv_out, dk_in, dv_in, one_src, two, line_src, lines,
+    kv_ref, qd_ref, g_ref, t_ref, k_raw, v_prev, kn, qn, q_unit, q_rms, k_unit, k_rms,
+    tiles, e_own, dp_own, dk_acc, dv_acc, out_ref, dk_in, dv_in, one_src, two, line_src, lines,
     load_sem, send_sem, recv_sem, red_sem, hand_sem,
 ):
-    heads, rows, _ = q_ref.shape
+    heads, rows, _ = k_raw.shape
+    k_ref, v_ref = kv_ref.at[pl.ds(0, heads)], kv_ref.at[pl.ds(heads, heads)]
+    q_ref, do_ref = qd_ref.at[pl.ds(0, heads)], qd_ref.at[pl.ds(heads, heads)]
+    dk_out, dv_out = out_ref.at[pl.ds(0, heads)], out_ref.at[pl.ds(heads, heads)]
     half = rows // 2
     entries = t_ref.shape[1]
     lead = SEG - 1
@@ -64,14 +71,16 @@
         return pltpu.make_async_copy(src, dst, load_sem.at[slot])
 
     def by_head(src, dst, slot):
-        return [load(src.at[:, pl.ds(h * HEAD_DIM, HEAD_DIM)], dst.at[h], slot + h) for h in range(heads)]
-
-    load_k = by_head(k_hbm, k_ref, 0)
-    load_v = by_head(v_hbm, v_ref, heads)
-    load_small = [load(t_hbm, t_ref, 4 * heads), load(g_hbm, g_ref, 4 * heads + 1)]
-    load_q = by_head(q_hbm, q_ref, 2 * heads)
-    load_do = by_head(do_hbm, do_ref, 3 * heads)
-    for copy in load_k + load_v + load_small + load_q + load_do:
+        return [load(src.at[:, pl.ds(h * HEAD_DIM, HEAD_DIM)], dst.at[h], slot) for h in range(heads)]
+
+    def drain(ref, sem):
+        pltpu.make_async_copy(ref, ref, sem).wait()
+
+    load_small = [load(t_hbm, t_ref, 2), load(g_hbm, g_ref, 3)]
+    for copy in (
+        by_head(k_hbm, k_ref, 0) + by_head(v_hbm, v_ref, 0) + load_small
+        + by_head(q_hbm, q_ref, 1) + by_head(do_hbm, do_ref, 1)
+    ):
         copy.start()
 
     def signal(sem, at, core):
@@ -107,7 +116,7 @@
 
     def send(slot, src, dst, to):
         return pltpu.make_async_remote_copy(
-            src_ref=src, dst_ref=dst, send_sem=send_sem.at[slot], recv_sem=recv_sem.at[slot],
+            src_ref=src, dst_ref=dst, send_sem=send_sem.at[slot % 4 // 2], recv_sem=recv_sem.at[slot],
             device_id=(to, tp), device_id_type=MESH,
         )
 
@@ -122,8 +131,7 @@
             for copy in copies:
                 copy.start()
 
-    for copy in load_k + load_v:
-        copy.wait()
+    drain(kv_ref, load_sem.at[0])
     yields = tp == n_tp - 1
     eager = sp < n_sp // 4
     start(has_next, [k_next[0], v_next[0]])
@@ -166,13 +174,13 @@
         tiles[h, 3] = (distant - top) * LOG2E + absent
         tiles[h, 4] = (before - top) * LOG2E + absent
 
+    inverse = 1.0 / g_ref[...]
     for h in range(heads):
         unit, rms = unit_of(k_ref[h])
         k_unit[h] = unit
         k_rms[h] = rms
         kn[h, rows:, :] = (unit * g1).astype(BF16)
-    for copy in load_q + load_do:
-        copy.wait()
+    drain(qd_ref, load_sem.at[1])
 
     sums = []
     for h in range(heads):
@@ -228,6 +236,8 @@
         dv_acc[h, high, :] = dot(e2.astype(BF16), d_o[high], (1, 0))
         if h == 0:
             start(has_next & yields, k_next[1:])
+        if h == heads - 1:
+            start(has_prev & jnp.logical_not(yields), [dv_back[h]])
         if step < len(rounds) - 1:
             step = relay(step)
         if h == 0:
@@ -259,10 +269,11 @@
             product = term if product is None else product + term
         mass = mass + jnp.sum(product, axis=0, keepdims=True)
         same, before = e0 + e2, x1 + e1
-        line_p = diagonals(jnp.where(upper, same, before), lead)
-        line_n = diagonals(jnp.where(upper, 0.0, same), lead)
+        fold_p = fold(jnp.where(upper, same, before), lead)
+        fold_n = fold(jnp.where(upper, 0.0, same), lead)
+        line_p, line_n = align(fold_p), align(fold_n)
         lane = lax.broadcasted_iota(jnp.int32, line_p.shape, 1)
-        rest = -(jnp.sum(line_p, axis=1, keepdims=True) + jnp.sum(line_n, axis=1, keepdims=True))
+        rest = -jnp.sum(jnp.sum(fold_p + fold_n, axis=0, keepdims=True), axis=1, keepdims=True)
         packed.append(jnp.where(lane < lead, line_n, line_p))
         packed.append(jnp.where(lane < lead, line_p, jnp.where(lane == lead, rest, 0.0)))
         dk_out[h, low, :] = d_k[0].astype(BF16)
@@ -314,7 +325,7 @@
             def _():
                 publish()
 
-            start(has_prev & jnp.logical_not(yields), [dk_back[h], dv_back[h]])
+            start(has_prev & jnp.logical_not(yields), [dk_back[h]])
         for i, part in enumerate([
             dot(jnp.concatenate([blocks[0], blocks[1][:, low], blocks[2][:, low]], axis=0), kn[h, 0 : 3 * half, :], (0, 0)),
             dot(jnp.concatenate([blocks[1][:, high], blocks[2][:, high], blocks[3]], axis=0), kn[h, half:, :], (0, 0)),
@@ -329,6 +340,8 @@
     def _():
         publish()
 
+    held = [dk_back[heads - 1], dv_back[heads - 1]]
+
     def add_dv(h):
         @pl.when(has_next)
         def _():
@@ -344,13 +357,16 @@
             (dv_back if h < heads - 1 else dk_back)[h].wait_recv()
 
         if h == 0:
-            start(has_prev & yields, [dk_back[heads - 1], dv_back[heads - 1]])
+            start(has_prev & yields & jnp.logical_not(eager), held)
         if h < heads - 1:
             add_dv(h)
 
             @pl.when(has_next)
             def _():
                 dk_back[h].wait_recv()
+
+        if h == 0:
+            start(has_prev & yields & eager, held)
 
         @pl.when(has_next)
         def _():
@@ -360,17 +376,10 @@
         grad = dk_acc[h] * factor * g1
         out = k_rms[h] * (grad - unit * jnp.mean(grad * unit, axis=-1, keepdims=True))
         dk_ref[:, across] = out.astype(BF16)
-        if h == heads - 1:
-            @pl.when(has_next)
-            def _():
-                dv_back[h].wait_recv()
-
-            add_dv(h)
-
-    inverse = 1.0 / g_ref[...]
+
     peers = two.at[pl.ds(0, n_sp - 1)]
-    pltpu.make_async_copy(peers, peers, red_sem.at[1]).wait()
-    pltpu.make_async_copy(lines, lines, red_sem.at[3]).wait()
+    drain(peers, red_sem.at[1])
+    drain(lines, red_sem.at[3])
     whole = jnp.sum(two[...], axis=0)
     for h in range(heads):
         dt_ref[h : h + 1, 0:half] = whole[2 * h : 2 * h + 1]
@@ -378,18 +387,19 @@
     mass = whole[2 * heads : 2 * heads + 1] + jnp.sum(lines[...], axis=(0, 1))
     dg_ref[...] = mass * inverse
 
-    pltpu.make_async_copy(peers, peers, red_sem.at[0]).wait()
-    pltpu.make_async_copy(lines, lines, red_sem.at[2]).wait()
+    drain(peers, red_sem.at[0])
+    drain(lines, red_sem.at[2])
+
+    @pl.when(has_prev)
+    def _():
+        drain(out_ref, send_sem.at[1])
 
     @pl.when(has_next)
     def _():
-        for copy in k_next + v_next:
-            copy.wait_send()
-
-    @pl.when(has_prev)
-    def _():
-        for copy in dv_back + dk_back:
-            copy.wait_send()
+        drain(kv_ref, send_sem.at[0])
+        dv_back[heads - 1].wait_recv()
+
+    add_dv(heads - 1)
 
 
 def emit(*refs):
@@ -418,6 +428,7 @@
             jax.ShapeDtypeStruct(gains.shape, F32),
         )
         low = pltpu.VMEM((heads, rows, HEAD_DIM), BF16)
+        pair = pltpu.VMEM((2 * heads, rows, HEAD_DIM), BF16)
         wide = pltpu.VMEM((heads, rows, HEAD_DIM), F32)
         thin = pltpu.VMEM((heads, rows, 1), F32)
         parts = pl.pallas_call(
@@ -426,7 +437,7 @@
             in_specs=[pl.BlockSpec(memory_space=pltpu.HBM)] * 6,
             out_specs=(vmem,) * 5,
             scratch_shapes=[
-                low, low, low, low,
+                pair, pair,
                 pltpu.VMEM(gains.shape, F32),
                 pltpu.VMEM(bias_table.shape[::-1], F32),
                 low, low,
@@ -437,13 +448,13 @@
                 pltpu.VMEM((heads, 3, half, half), F32),
                 pltpu.VMEM((heads, 3, half, half), F32),
                 wide, wide,
-                low, low, low, low,
+                pair, low, low,
                 pltpu.VMEM((8, HEAD_DIM), F32),
                 pltpu.VMEM((n_sp, 8, HEAD_DIM), F32),
                 pltpu.VMEM((1, HEAD_DIM), F32),
                 pltpu.VMEM((n_tp - 1, n_sp, 1, HEAD_DIM), F32),
-                pltpu.SemaphoreType.DMA((4 * heads + 2,)),
-                pltpu.SemaphoreType.DMA((4 * heads,)),
+                pltpu.SemaphoreType.DMA((4,)),
+                pltpu.SemaphoreType.DMA((2,)),
                 pltpu.SemaphoreType.DMA((4 * heads,)),
                 pltpu.SemaphoreType.DMA((4,)),
                 pltpu.SemaphoreType.REGULAR((max(1, (n_sp - 1).bit_length()),)),

time: 19.1 us -> 18.8 us (0.984)
  no operation moved by 1% of the time
where the time goes in v4:
time: 18.8 us; the launch traced here: 18.6 us
  Pallas kernels  18 us (96%)
  between operations  0.64 us (3%)
    pallas_call x1, Pallas kernels, local(): pl.pallas_call(functools.partial(kernel, n_sp, n_tp), out_shape=shapes, i...  17.2 us
    pallas_call x1, Pallas kernels, local(): pl.pallas_call(emit, out_shape=shapes, in_specs=[vmem] * 5, out_specs=(pl...  0.79 us

profile of v4, /device:TPU:0, one launch (start us, length us, event | category | flops | bytes accessed | tf_op | source)
XLA Modules:
  0.0 18.6 jit_solution(17448503899626331744)
XLA Ops:
  0.6 17.2 %shard_map.101 = (bf16[256,256]{1,0:T(8,128)(2,1)S(1)}, bf16[256,256]{1,0:T(8,128)(2,1)S(1)}, bf16[256,256]{1,0:T(8,128)(2,1)S(1)}, f32[2,192]{1,0:T(2,128)S(1)}, f32[2,128]{1,0:T(2,128)S(1)}) custom-call(bf16[256,256]{1,0:T(8,128)(2,1)} %q_hbm.1, bf16[256,256]{1,0:T(8,128)(2,1)} %k_hbm.1, bf16[256,256]{1,0:T(8,128)(2,1)} %v_hbm.1, bf16[256,256]{1,0:T(8,128)(2,1)} %do_hbm.1, ...), custom_call_target="tpu_custom_call" | custom-call | tf_op jit(solution)/shard_map/pallas_call | solution.py:434
  17.8 0.8 %shard_map.102 = (bf16[256,256]{1,0:T(8,128)(2,1)}, bf16[256,256]{1,0:T(8,128)(2,1)}, bf16[256,256]{1,0:T(8,128)(2,1)}, f32[2,192]{1,0:T(2,128)}, f32[2,128]{1,0:T(2,128)}) custom-call(bf16[256,256]{1,0:T(8,128)(2,1)S(1)} %get-tuple-element.15.refs_0_, bf16[256,256]{1,0:T(8,128)(2,1)S(1)} %get-tuple-element.16.refs_1_, ...), custom_call_target="tpu_custom_call" | custom-call | tf_op jit(solution)/shard_map/pallas_call | solution.py:469

commit v5 on v4

--- a/solution.py
+++ b/solution.py
@@ -76,6 +76,25 @@
     def drain(ref, sem):
         pltpu.make_async_copy(ref, ref, sem).wait()
 
+    def signal(sem, at, core):
+        pl.semaphore_signal(sem, inc=1, device_id=(at, core), device_id_type=MESH)
+
+    def around(sem, radius):
+        @pl.when(sp >= radius)
+        def _():
+            signal(sem, sp - radius, tp)
+
+        @pl.when(sp < n_sp - radius)
+        def _():
+            signal(sem, sp + radius, tp)
+
+    def count_around(radius):
+        return jnp.where(sp >= radius, 1, 0) + jnp.where(sp < n_sp - radius, 1, 0)
+
+    barrier = pltpu.get_barrier_semaphore()
+    around(barrier, 1)
+    for other in range(1, n_tp):
+        signal(barrier, sp, lax.rem(tp + other, n_tp))
     load_small = [load(t_hbm, t_ref, 2), load(g_hbm, g_ref, 3)]
     for copy in (
         by_head(k_hbm, k_ref, 0) + by_head(v_hbm, v_ref, 0) + load_small
@@ -83,25 +102,6 @@
     ):
         copy.start()
 
-    def signal(sem, at, core):
-        pl.semaphore_signal(sem, inc=1, device_id=(at, core), device_id_type=MESH)
-
-    def around(sem, radius):
-        @pl.when(sp >= radius)
-        def _():
-            signal(sem, sp - radius, tp)
-
-        @pl.when(sp < n_sp - radius)
-        def _():
-            signal(sem, sp + radius, tp)
-
-    def count_around(radius):
-        return jnp.where(sp >= radius, 1, 0) + jnp.where(sp < n_sp - radius, 1, 0)
-
-    barrier = pltpu.get_barrier_semaphore()
-    around(barrier, 1)
-    for other in range(1, n_tp):
-        signal(barrier, sp, lax.rem(tp + other, n_tp))
     pl.semaphore_wait(barrier, count_around(1) + n_tp - 1)
 
     rounds = []
@@ -234,14 +234,10 @@
         dv_out[h, high, :] = dot(jnp.concatenate([x1, x2], axis=1).astype(BF16), d_o, (1, 0)).astype(BF16)
         dv_acc[h, low, :] = dot(jnp.concatenate([e0, e1], axis=1).astype(BF16), d_o, (1, 0))
         dv_acc[h, high, :] = dot(e2.astype(BF16), d_o[high], (1, 0))
-        if h == 0:
-            start(has_next & yields, k_next[1:])
         if h == heads - 1:
             start(has_prev & jnp.logical_not(yields), [dv_back[h]])
         if step < len(rounds) - 1:
             step = relay(step)
-        if h == 0:
-            start(has_next & yields, v_next[1:])
         own0 = jnp.sum(e0 * dp_own[h, 0], axis=0, keepdims=True)
         own1 = jnp.sum(e1 * dp_own[h, 1] + e2 * dp_own[h, 2], axis=0, keepdims=True)
 
@@ -249,6 +245,8 @@
         def _():
             v_next[h].wait_recv()
 
+        if h == 0:
+            start(has_next & yields, k_next[1:] + v_next[1:])
         p0 = dot(v_prev[h, low, :], d_o[low], (1, 1))
         p1 = dot(v_prev[h, high, :], d_o, (1, 1))
         delta0 = own0 + jnp.sum(x0 * p0 + x1 * p1[:, low], axis=0, keepdims=True)
@@ -356,8 +354,6 @@
         def _():
             (dv_back if h < heads - 1 else dk_back)[h].wait_recv()
 
-        if h == 0:
-            start(has_prev & yields & jnp.logical_not(eager), held)
         if h < heads - 1:
             add_dv(h)
 
@@ -366,7 +362,7 @@
                 dk_back[h].wait_recv()
 
         if h == 0:
-            start(has_prev & yields & eager, held)
+            start(has_prev & yields, held)
 
         @pl.when(has_next)
         def _():

time: 18.8 us -> 18.6 us (0.989)
  Pallas kernels: 18 us -> 17.8 us
where the time goes in v5:
time: 18.6 us; the launch traced here: 18.5 us
  Pallas kernels  17.8 us (96%)
  between operations  0.64 us (3%)
    pallas_call x1, Pallas kernels, local(): pl.pallas_call(functools.partial(kernel, n_sp, n_tp), out_shape=shapes, i...  17 us
    pallas_call x1, Pallas kernels, local(): pl.pallas_call(emit, out_shape=shapes, in_specs=[vmem] * 5, out_specs=(pl...  0.79 us

profile of v5, /device:TPU:0, one launch (start us, length us, event | category | flops | bytes accessed | tf_op | source)
XLA Modules:
  0.0 18.5 jit_solution(3266890981666515902)
XLA Ops:
  0.6 17.0 %shard_map.101 = (bf16[256,256]{1,0:T(8,128)(2,1)S(1)}, bf16[256,256]{1,0:T(8,128)(2,1)S(1)}, bf16[256,256]{1,0:T(8,128)(2,1)S(1)}, f32[2,192]{1,0:T(2,128)S(1)}, f32[2,128]{1,0:T(2,128)S(1)}) custom-call(bf16[256,256]{1,0:T(8,128)(2,1)} %q_hbm.1, bf16[256,256]{1,0:T(8,128)(2,1)} %k_hbm.1, bf16[256,256]{1,0:T(8,128)(2,1)} %v_hbm.1, bf16[256,256]{1,0:T(8,128)(2,1)} %do_hbm.1, ...), custom_call_target="tpu_custom_call" | custom-call | tf_op jit(solution)/shard_map/pallas_call | solution.py:430
  17.7 0.8 %shard_map.102 = (bf16[256,256]{1,0:T(8,128)(2,1)}, bf16[256,256]{1,0:T(8,128)(2,1)}, bf16[256,256]{1,0:T(8,128)(2,1)}, f32[2,192]{1,0:T(2,128)}, f32[2,128]{1,0:T(2,128)}) custom-call(bf16[256,256]{1,0:T(8,128)(2,1)S(1)} %get-tuple-element.15.refs_0_, bf16[256,256]{1,0:T(8,128)(2,1)S(1)} %get-tuple-element.16.refs_1_, ...), custom_call_target="tpu_custom_call" | custom-call | tf_op jit(solution)/shard_map/pallas_call | solution.py:465

commit v6 on v5

--- a/solution.py
+++ b/solution.py
@@ -52,7 +52,7 @@
     dq_ref, dk_ref, dv_ref, dt_ref, dg_ref,
     kv_ref, qd_ref, g_ref, t_ref, k_raw, v_prev, kn, qn, q_unit, q_rms, k_unit, k_rms,
     tiles, e_own, dp_own, dk_acc, dv_acc, out_ref, dk_in, dv_in, one_src, two, line_src, lines,
-    load_sem, send_sem, recv_sem, red_sem, hand_sem,
+    load_sem, recv_sem, red_sem, hand_sem,
 ):
     heads, rows, _ = k_raw.shape
     k_ref, v_ref = kv_ref.at[pl.ds(0, heads)], kv_ref.at[pl.ds(heads, heads)]
@@ -116,7 +116,7 @@
 
     def send(slot, src, dst, to):
         return pltpu.make_async_remote_copy(
-            src_ref=src, dst_ref=dst, send_sem=send_sem.at[slot % 4 // 2], recv_sem=recv_sem.at[slot],
+            src_ref=src, dst_ref=dst, send_sem=load_sem.at[slot % 4 // 2], recv_sem=recv_sem.at[slot],
             device_id=(to, tp), device_id_type=MESH,
         )
 
@@ -291,15 +291,15 @@
             def spread(i):
                 at = jnp.where(i >= sp, i + 1, i)
                 pltpu.make_async_remote_copy(
-                    src_ref=one_src, dst_ref=two.at[sp], send_sem=red_sem.at[0], recv_sem=red_sem.at[1],
+                    src_ref=one_src, dst_ref=two.at[sp], send_sem=load_sem.at[2], recv_sem=red_sem.at[0],
                     device_id=(at, tp), device_id_type=MESH,
                 ).start()
 
             def spread_line(at):
                 for other in range(1, n_tp):
                     pltpu.make_async_remote_copy(
-                        src_ref=line_src, dst_ref=lines.at[other - 1, sp], send_sem=red_sem.at[2],
-                        recv_sem=red_sem.at[3], device_id=(at, lax.rem(tp + other, n_tp)), device_id_type=MESH,
+                        src_ref=line_src, dst_ref=lines.at[other - 1, sp], send_sem=load_sem.at[3],
+                        recv_sem=red_sem.at[1], device_id=(at, lax.rem(tp + other, n_tp)), device_id_type=MESH,
                     ).start()
 
             def publish():
@@ -347,8 +347,20 @@
 
         dv_ref[:, h * HEAD_DIM : (h + 1) * HEAD_DIM] = dv_acc[h].astype(BF16)
 
+    def finish_dv():
+        @pl.when(has_next)
+        def _():
+            dv_back[heads - 1].wait_recv()
+
+        add_dv(heads - 1)
+
     for h in range(heads):
         across = slice(h * HEAD_DIM, (h + 1) * HEAD_DIM)
+
+        if h == heads - 1:
+            @pl.when(jnp.logical_not(yields))
+            def _():
+                finish_dv()
 
         @pl.when(has_next)
         def _():
@@ -374,8 +386,8 @@
         dk_ref[:, across] = out.astype(BF16)
 
     peers = two.at[pl.ds(0, n_sp - 1)]
-    drain(peers, red_sem.at[1])
-    drain(lines, red_sem.at[3])
+    drain(peers, red_sem.at[0])
+    drain(lines, red_sem.at[1])
     whole = jnp.sum(two[...], axis=0)
     for h in range(heads):
         dt_ref[h : h + 1, 0:half] = whole[2 * h : 2 * h + 1]
@@ -383,19 +395,20 @@
     mass = whole[2 * heads : 2 * heads + 1] + jnp.sum(lines[...], axis=(0, 1))
     dg_ref[...] = mass * inverse
 
-    drain(peers, red_sem.at[0])
-    drain(lines, red_sem.at[2])
+    drain(peers, load_sem.at[2])
+    drain(lines, load_sem.at[3])
 
     @pl.when(has_prev)
     def _():
-        drain(out_ref, send_sem.at[1])
+        drain(out_ref, load_sem.at[1])
 
     @pl.when(has_next)
     def _():
-        drain(kv_ref, send_sem.at[0])
-        dv_back[heads - 1].wait_recv()
-
-    add_dv(heads - 1)
+        drain(kv_ref, load_sem.at[0])
+
+    @pl.when(yields)
+    def _():
+        finish_dv()
 
 
 def emit(*refs):
@@ -450,9 +463,8 @@
                 pltpu.VMEM((1, HEAD_DIM), F32),
                 pltpu.VMEM((n_tp - 1, n_sp, 1, HEAD_DIM), F32),
                 pltpu.SemaphoreType.DMA((4,)),
+                pltpu.SemaphoreType.DMA((4 * heads,)),
                 pltpu.SemaphoreType.DMA((2,)),
-                pltpu.SemaphoreType.DMA((4 * heads,)),
-                pltpu.SemaphoreType.DMA((4,)),
                 pltpu.SemaphoreType.REGULAR((max(1, (n_sp - 1).bit_length()),)),
             ],
             compiler_params=pltpu.CompilerParams(

time: 18.6 us -> 18.6 us (level)
  no operation moved by 1% of the time
where the time goes in v6:
time: 18.6 us; the launch traced here: 18.4 us
  Pallas kernels  17.8 us (96%)
  between operations  0.64 us (3%)
    pallas_call x1, Pallas kernels, local(): pl.pallas_call(functools.partial(kernel, n_sp, n_tp), out_shape=shapes, i...  17 us
    pallas_call x1, Pallas kernels, local(): pl.pallas_call(emit, out_shape=shapes, in_specs=[vmem] * 5, out_specs=(pl...  0.79 us

profile of v6, /device:TPU:0, one launch (start us, length us, event | category | flops | bytes accessed | tf_op | source)
XLA Modules:
  0.0 18.4 jit_solution(4848535273659426781)
XLA Ops:
  0.6 17.0 %shard_map.101 = (bf16[256,256]{1,0:T(8,128)(2,1)S(1)}, bf16[256,256]{1,0:T(8,128)(2,1)S(1)}, bf16[256,256]{1,0:T(8,128)(2,1)S(1)}, f32[2,192]{1,0:T(2,128)S(1)}, f32[2,128]{1,0:T(2,128)S(1)}) custom-call(bf16[256,256]{1,0:T(8,128)(2,1)} %q_hbm.1, bf16[256,256]{1,0:T(8,128)(2,1)} %k_hbm.1, bf16[256,256]{1,0:T(8,128)(2,1)} %v_hbm.1, bf16[256,256]{1,0:T(8,128)(2,1)} %do_hbm.1, ...), custom_call_target="tpu_custom_call" | custom-call | tf_op jit(solution)/shard_map/pallas_call | solution.py:443
  17.6 0.8 %shard_map.102 = (bf16[256,256]{1,0:T(8,128)(2,1)}, bf16[256,256]{1,0:T(8,128)(2,1)}, bf16[256,256]{1,0:T(8,128)(2,1)}, f32[2,192]{1,0:T(2,128)}, f32[2,128]{1,0:T(2,128)}) custom-call(bf16[256,256]{1,0:T(8,128)(2,1)S(1)} %get-tuple-element.15.refs_0_, bf16[256,256]{1,0:T(8,128)(2,1)S(1)} %get-tuple-element.16.refs_1_, ...), custom_call_target="tpu_custom_call" | custom-call | tf_op jit(solution)/shard_map/pallas_call | solution.py:477

commit v7 on v6

--- a/solution.py
+++ b/solution.py
@@ -386,6 +386,17 @@
         dk_ref[:, across] = out.astype(BF16)
 
     peers = two.at[pl.ds(0, n_sp - 1)]
+    drain(peers, load_sem.at[2])
+    drain(lines, load_sem.at[3])
+
+    @pl.when(has_prev)
+    def _():
+        drain(out_ref, load_sem.at[1])
+
+    @pl.when(has_next)
+    def _():
+        drain(kv_ref, load_sem.at[0])
+
     drain(peers, red_sem.at[0])
     drain(lines, red_sem.at[1])
     whole = jnp.sum(two[...], axis=0)
@@ -394,17 +405,6 @@
         dt_ref[h : h + 1, half:] = whole[2 * h + 1 : 2 * h + 2, 0 : entries - half]
     mass = whole[2 * heads : 2 * heads + 1] + jnp.sum(lines[...], axis=(0, 1))
     dg_ref[...] = mass * inverse
-
-    drain(peers, load_sem.at[2])
-    drain(lines, load_sem.at[3])
-
-    @pl.when(has_prev)
-    def _():
-        drain(out_ref, load_sem.at[1])
-
-    @pl.when(has_next)
-    def _():
-        drain(kv_ref, load_sem.at[0])
 
     @pl.when(yields)
     def _():

time: 18.6 us -> 18.5 us (level)
  no operation moved by 1% of the time
where the time goes in v7:
time: 18.5 us; the launch traced here: 18.4 us
  Pallas kernels  17.8 us (96%)
  between operations  0.64 us (3%)
    pallas_call x1, Pallas kernels, local(): pl.pallas_call(functools.partial(kernel, n_sp, n_tp), out_shape=shapes, i...  17 us
    pallas_call x1, Pallas kernels, local(): pl.pallas_call(emit, out_shape=shapes, in_specs=[vmem] * 5, out_specs=(pl...  0.79 us

profile of v7, /device:TPU:0, one launch (start us, length us, event | category | flops | bytes accessed | tf_op | source)
XLA Modules:
  0.0 18.4 jit_solution(12071228589646730019)
XLA Ops:
  0.6 17.0 %shard_map.101 = (bf16[256,256]{1,0:T(8,128)(2,1)S(1)}, bf16[256,256]{1,0:T(8,128)(2,1)S(1)}, bf16[256,256]{1,0:T(8,128)(2,1)S(1)}, f32[2,192]{1,0:T(2,128)S(1)}, f32[2,128]{1,0:T(2,128)S(1)}) custom-call(bf16[256,256]{1,0:T(8,128)(2,1)} %q_hbm.1, bf16[256,256]{1,0:T(8,128)(2,1)} %k_hbm.1, bf16[256,256]{1,0:T(8,128)(2,1)} %v_hbm.1, bf16[256,256]{1,0:T(8,128)(2,1)} %do_hbm.1, ...), custom_call_target="tpu_custom_call" | custom-call | tf_op jit(solution)/shard_map/pallas_call | solution.py:443
  17.6 0.8 %shard_map.102 = (bf16[256,256]{1,0:T(8,128)(2,1)}, bf16[256,256]{1,0:T(8,128)(2,1)}, bf16[256,256]{1,0:T(8,128)(2,1)}, f32[2,192]{1,0:T(2,128)}, f32[2,128]{1,0:T(2,128)}) custom-call(bf16[256,256]{1,0:T(8,128)(2,1)S(1)} %get-tuple-element.15.refs_0_, bf16[256,256]{1,0:T(8,128)(2,1)S(1)} %get-tuple-element.16.refs_1_, ...), custom_call_target="tpu_custom_call" | custom-call | tf_op jit(solution)/shard_map/pallas_call | solution.py:477

commit v8 on v6

--- a/solution.py
+++ b/solution.py
@@ -234,8 +234,7 @@
         dv_out[h, high, :] = dot(jnp.concatenate([x1, x2], axis=1).astype(BF16), d_o, (1, 0)).astype(BF16)
         dv_acc[h, low, :] = dot(jnp.concatenate([e0, e1], axis=1).astype(BF16), d_o, (1, 0))
         dv_acc[h, high, :] = dot(e2.astype(BF16), d_o[high], (1, 0))
-        if h == heads - 1:
-            start(has_prev & jnp.logical_not(yields), [dv_back[h]])
+        start(has_prev & jnp.logical_not(yields), [dv_back[h]])
         if step < len(rounds) - 1:
             step = relay(step)
         own0 = jnp.sum(e0 * dp_own[h, 0], axis=0, keepdims=True)
@@ -279,7 +278,8 @@
         dk_acc[h, low, :] = d_k[2]
         dk_acc[h, high, :] = d_k[3]
         if h < heads - 1:
-            start(has_prev, [dv_back[h], dk_back[h]])
+            start(has_prev & yields, [dv_back[h]])
+            start(has_prev, [dk_back[h]])
         else:
             mass = mass * factor
             line_src[...] = mass

time: 18.6 us -> 19.1 us (1.027)
  the two profiles are of different devices: /device:TPU:0 before, /device:TPU:1 now
where the time goes in v8:
time: 19.1 us; the launch traced here: 18.9 us
  Pallas kernels  18.3 us (96%)
  between operations  0.64 us (3%)
    pallas_call x1, Pallas kernels, local(): pl.pallas_call(functools.partial(kernel, n_sp, n_tp), out_shape=shapes, i...  17.5 us
    pallas_call x1, Pallas kernels, local(): pl.pallas_call(emit, out_shape=shapes, in_specs=[vmem] * 5, out_specs=(pl...  0.79 us

profile of v8, /device:TPU:1, one launch (start us, length us, event | category | flops | bytes accessed | tf_op | source)
XLA Modules:
  0.0 18.9 jit_solution(48446822532802518)
XLA Ops:
  0.6 17.5 %shard_map.101 = (bf16[256,256]{1,0:T(8,128)(2,1)S(1)}, bf16[256,256]{1,0:T(8,128)(2,1)S(1)}, bf16[256,256]{1,0:T(8,128)(2,1)S(1)}, f32[2,192]{1,0:T(2,128)S(1)}, f32[2,128]{1,0:T(2,128)S(1)}) custom-call(bf16[256,256]{1,0:T(8,128)(2,1)} %q_hbm.1, bf16[256,256]{1,0:T(8,128)(2,1)} %k_hbm.1, bf16[256,256]{1,0:T(8,128)(2,1)} %v_hbm.1, bf16[256,256]{1,0:T(8,128)(2,1)} %do_hbm.1, ...), custom_call_target="tpu_custom_call" | custom-call | tf_op jit(solution)/shard_map/pallas_call | solution.py:443
  18.1 0.8 %shard_map.102 = (bf16[256,256]{1,0:T(8,128)(2,1)}, bf16[256,256]{1,0:T(8,128)(2,1)}, bf16[256,256]{1,0:T(8,128)(2,1)}, f32[2,192]{1,0:T(2,128)}, f32[2,128]{1,0:T(2,128)}) custom-call(bf16[256,256]{1,0:T(8,128)(2,1)S(1)} %get-tuple-element.15.refs_0_, bf16[256,256]{1,0:T(8,128)(2,1)S(1)} %get-tuple-element.16.refs_1_, ...), custom_call_target="tpu_custom_call" | custom-call | tf_op jit(solution)/shard_map/pallas_call | solution.py:477
